TPU v7x, 32 devices: a whole 2x2x4 slice. The times are simulated.
32 devices in a mesh: rep: 4 (over z), fs: 4 (over y, x), tp: 2 (over core).
Axes of the slice: x: 2, y: 2, z: 4, core: 2. Of those that a mesh axis runs over, the one named last changes fastest.
Arguments:
- inputs: bfloat16 [512, 2048], P(('rep', 'fs', 'tp')), may hold values from -6 to 6
- cotangent: bfloat16 [512, 2048], P(('rep', 'fs', 'tp')), may hold values from -6 to 6
- norm_gain: float32 [2048], replicated, may hold values from 0.1 to 1.9
- gate_weight: bfloat16 [2048, 2816], P(None, ('fs', 'tp')), may hold values from -0.125 to 0.125
- up_weight: bfloat16 [2048, 2816], P(None, ('fs', 'tp')), may hold values from -0.125 to 0.125
- down_weight: bfloat16 [2816, 2048], P(('fs', 'tp')), may hold values from -0.109375 to 0.109375
Outputs:
- input_grad: bfloat16 [512, 2048], P(('rep', 'fs', 'tp'))
- gain_grad: float32 [2048], replicated
- down_grad: float32 [2816, 2048], P(('fs', 'tp'), 'rep')
All inputs are finite; a program needn't handle non-finite values.
Results may differ from a plain program's by a relative error of at most 0.0066.
Values may be sent and summed in bfloat16 or wider, within the bound.
A program may use at most 64 MiB of HBM per device.

v0:
```python
import functools

import jax
import jax.numpy as jnp
from jax import lax
from jax.experimental import pallas as pl
from jax.experimental.pallas import tpu as pltpu
from jax.sharding import PartitionSpec as P

EPS = 1e-06


def across_tokens(left, right):
    return lax.dot_general(
        left, right, (((0,), (0,)), ((), ())), preferred_element_type=jnp.float32
    )


def across_columns(left, right):
    return lax.dot_general(
        left, right, (((1,), (1,)), ((), ())), preferred_element_type=jnp.float32
    )


def per_device(inputs, cotangent, norm_gain, gate_weight, up_weight, down_weight):
    whole_x, whole_dy = (
        lax.all_gather(inputs, ("fs", "tp"), axis=0, tiled=True),
        lax.all_gather(cotangent, ("fs", "tp"), axis=0, tiled=True),
    )
    xf = whole_x.astype(jnp.float32)
    inv = lax.rsqrt(jnp.mean(xf * xf, axis=-1, keepdims=True) + EPS)
    normed = xf * inv
    hidden_in = (normed * norm_gain).astype(jnp.bfloat16)
    gate = jnp.dot(hidden_in, gate_weight, preferred_element_type=jnp.float32)
    up = jnp.dot(hidden_in, up_weight, preferred_element_type=jnp.float32)
    sig = jax.nn.sigmoid(gate)
    act = gate * sig
    hidden = (act * up).astype(jnp.bfloat16)
    d_hidden = 0.5 * across_columns(whole_dy, down_weight)
    d_gate = (d_hidden * up * sig * (1.0 + gate * (1.0 - sig))).astype(jnp.bfloat16)
    d_up = (d_hidden * act).astype(jnp.bfloat16)
    own_rows = inputs.shape[0]
    d_in = lax.psum_scatter(
        across_columns(d_gate, gate_weight) + across_columns(d_up, up_weight),
        ("fs", "tp"),
        scatter_dimension=0,
        tiled=True,
    )
    offset = lax.axis_index(("fs", "tp")) * own_rows
    own_normed = lax.dynamic_slice_in_dim(normed, offset, own_rows, 0)
    own_inv = lax.dynamic_slice_in_dim(inv, offset, own_rows, 0)
    gain_grad = lax.psum(jnp.sum(d_in * own_normed, axis=0), ("rep", "fs", "tp"))
    scaled = d_in * norm_gain
    input_grad = (
        own_inv * (scaled - own_normed * jnp.mean(scaled * own_normed, axis=-1, keepdims=True))
    ).astype(jnp.bfloat16)
    input_grad, gain_grad = (input_grad, gain_grad)
    part_down = 0.5 * across_tokens(whole_dy, hidden)
    got_down = lax.all_to_all(
        part_down[None].astype(jnp.bfloat16), "rep", split_axis=1, concat_axis=0, tiled=True
    ).astype(jnp.float32)
    down_grad = jnp.sum(got_down, axis=0).T
    return (input_grad, gain_grad, down_grad)


MESH = pl.DeviceIdType.MESH
LANES = 128
PIECES = 4


def kernel(
    nr, nf,
    x_hbm, dy_hbm, gain_hbm, wg_hbm, wu_hbm, wd_hbm,
    dx_ref, dgain_ref, ddown_ref,
    x_ref, dy_ref, gain_ref, wg, wu, wd, xg, dyg, dyc, own_hid, hid, normed, d_in, d_out, d_pair, d_send, d_got, gz_own, gz, gg_own, gg,
    w_sem, x_s, x_r, xs_s, xs_r, y_s, y_r, ys_s, ys_r, cz_s, cz_r, c_s, c_r, cs_s, cs_r,
    h_s, h_r, p_s, p_r, d_s, d_r, gz_s, gz_r, gg_s, gg_r,
):
    r, f, t = lax.axis_index("rep"), lax.axis_index("fs"), lax.axis_index("tp")
    ng = 2 * nf
    me = 2 * f + t
    own, width = x_hbm.shape
    cols = ddown_ref.shape[1]
    sibling = (r, f, 1 - t)

    def chip(k):
        return lax.rem(f + k + nf, nf)

    def layer(k):
        return lax.rem(r + k + nr, nr)

    def member(k):
        g = lax.rem(me + k + ng, ng)
        return g, (r, g // 2, lax.rem(g, 2))

    def rows(g):
        return pl.ds(pl.multiple_of(g * own, own), own)

    def span(p):
        return pl.ds(pl.multiple_of(p * cols, LANES), cols)

    sent = []

    def send(src, dst, ssem, rsem, to):
        copy = pltpu.make_async_remote_copy(
            src_ref=src, dst_ref=dst, send_sem=ssem, recv_sem=rsem,
            device_id=to, device_id_type=MESH,
        )
        copy.start()
        sent.append(copy)

    def arrived(dst, ssem, rsem):
        pltpu.make_async_remote_copy(
            src_ref=dst, dst_ref=dst, send_sem=ssem, recv_sem=rsem,
            device_id=sibling, device_id_type=MESH,
        ).wait_recv()

    loads = [
        pltpu.make_async_copy(src, dst, w_sem.at[i])
        for i, (src, dst) in enumerate(
            (
                (x_hbm, x_ref), (dy_hbm, dy_ref), (gain_hbm, gain_ref),
                (wg_hbm, wg), (wu_hbm, wu), (wd_hbm, wd),
            )
        )
    ]
    for load in loads:
        load.start()

    barrier = pltpu.get_barrier_semaphore()
    for k in range(1, ng):
        pl.semaphore_signal(barrier, inc=1, device_id=member(k)[1], device_id_type=MESH)
    for k in range(1, nr):
        pl.semaphore_signal(barrier, inc=1, device_id=(layer(k), f, t), device_id_type=MESH)
    pl.semaphore_wait(barrier, ng - 1 + nr - 1)
    for load in loads[:3]:
        load.wait()

    for src, dst, ss, rs, bs, br in (
        (x_ref, xg, x_s, x_r, xs_s, xs_r), (dy_ref, dyg, y_s, y_r, ys_s, ys_r)
    ):
        for k in range(1, nf):
            send(src, dst.at[rows(me)], ss.at[k - 1], rs.at[k - 1], (r, chip(k), t))
        send(src, dst.at[rows(me)], bs.at[0], br.at[0], sibling)
    for k in range(1, nr):
        to = layer(k)
        send(
            dy_ref.at[:, span(to)], dyc.at[k - 1, rows(me)],
            cz_s.at[k - 1], cz_r.at[k - 1], (to, f, t),
        )
    xg[rows(me), :] = x_ref[...]
    dyg[rows(me), :] = dy_ref[...]

    def hand_on(ref, at, ss, rs, bs, br):
        for k in range(1, nf):
            block = at(ref, 2 * chip(-k) + t)
            arrived(block, ss.at[k - 1], rs.at[k - 1])
            send(block, block, bs.at[k], br.at[k], sibling)

    def from_sibling(ref, at, bs, br):
        for k in range(nf):
            arrived(at(ref, 2 * chip(-k) + 1 - t), bs.at[k], br.at[k])

    def plain(ref, g):
        return ref.at[rows(g)]

    def stacked(ref, g):
        return ref.at[:, rows(g)]

    hand_on(xg, plain, x_s, x_r, xs_s, xs_r)
    from_sibling(xg, plain, xs_s, xs_r)

    xf = xg[...].astype(jnp.float32)
    inv = lax.rsqrt(jnp.mean(xf * xf, axis=-1, keepdims=True) + EPS)
    normed[...] = xf * inv
    hidden_in = (normed[...] * gain_ref[...]).astype(jnp.bfloat16)
    for load in loads[3:]:
        load.wait()
    gate = across_columns(hidden_in, wg[...])
    up = across_columns(hidden_in, wu[...])

    sig = jax.nn.sigmoid(gate)
    act = gate * sig
    own_hid[...] = (act * up).astype(jnp.bfloat16)
    for k in range(1, nr):
        send(own_hid, hid.at[k - 1], h_s.at[k - 1], h_r.at[k - 1], (layer(k), f, t))

    hand_on(dyg, plain, y_s, y_r, ys_s, ys_r)
    for k in range(1, nr):
        arrived(dyc.at[k - 1, rows(me)], cz_s.at[k - 1], cz_r.at[k - 1])
    for k in range(1, nf):
        send(stacked(dyc, me), stacked(dyc, me), c_s.at[k - 1], c_r.at[k - 1], (r, chip(k), t))
    send(stacked(dyc, me), stacked(dyc, me), cs_s.at[0], cs_r.at[0], sibling)
    from_sibling(dyg, plain, ys_s, ys_r)
    d_hidden = 0.5 * across_columns(dyg[...], wd[...])
    d_gate = (d_hidden * up * sig * (1.0 + gate * (1.0 - sig))).astype(jnp.bfloat16)
    d_up = (d_hidden * act).astype(jnp.bfloat16)

    step = width // PIECES
    for p in range(PIECES):
        part = slice(p * step, (p + 1) * step)
        d_in[:, part] = jnp.dot(
            d_gate, wg[:, part], preferred_element_type=jnp.float32
        ) + jnp.dot(d_up, wu[:, part], preferred_element_type=jnp.float32)
        d_out[:, :, :, part] = (
            d_in[:, part].astype(jnp.bfloat16).reshape(nf, 2, own, step)
        )
        gg_own[:, part] = jnp.sum(d_in[:, part] * normed[:, part], axis=0, keepdims=True)
        send(
            d_out.at[:, 1 - t, :, part], d_pair.at[:, :, part], p_s.at[p], p_r.at[p], sibling
        )
    for k in range(1, ng):
        send(gg_own, gg.at[me], gg_s.at[k - 1], gg_r.at[k - 1], member(k)[1])
    gg[me] = gg_own[...]

    for p in range(PIECES):
        part = slice(p * step, (p + 1) * step)
        arrived(d_pair.at[:, :, part], p_s.at[p], p_r.at[p])
        for k in range(1, nf):
            to = chip(k)
            d_send[k - 1, :, part] = (
                d_in[rows(2 * to + t), part] + d_pair[to, :, part].astype(jnp.float32)
            ).astype(jnp.bfloat16)
            send(
                d_send.at[k - 1, :, part], d_got.at[k - 1, :, part],
                d_s.at[p, k - 1], d_r.at[p, k - 1], (r, to, t),
            )

    hand_on(dyc, stacked, c_s, c_r, cs_s, cs_r)
    for k in range(1, ng):
        arrived(gg.at[member(-k)[0]], gg_s.at[k - 1], gg_r.at[k - 1])
    gz_own[...] = jnp.sum(gg[...], axis=0)
    for k in range(1, nr):
        send(gz_own, gz.at[r], gz_s.at[k - 1], gz_r.at[k - 1], (layer(k), f, t))
    gz[r] = gz_own[...]
    total = across_tokens(own_hid[...], dyg[:, span(r)])

    from_sibling(dyc, stacked, cs_s, cs_r)
    for k in range(1, nr):
        arrived(hid.at[k - 1], h_s.at[k - 1], h_r.at[k - 1])
        total = total + across_tokens(hid[k - 1], dyc[k - 1])
    ddown_ref[...] = 0.5 * total

    mine = d_in[rows(me), :] + d_pair[f].astype(jnp.float32)
    for k in range(1, nf):
        for p in range(PIECES):
            arrived(
                d_got.at[k - 1, :, slice(p * step, (p + 1) * step)],
                d_s.at[p, k - 1], d_r.at[p, k - 1],
            )
        mine = mine + d_got[k - 1].astype(jnp.float32)
    xf = x_ref[...].astype(jnp.float32)
    own_inv = lax.rsqrt(jnp.mean(xf * xf, axis=-1, keepdims=True) + EPS)
    own_normed = xf * own_inv
    scaled = mine * gain_ref[...]
    dx_ref[...] = (
        own_inv * (scaled - own_normed * jnp.mean(scaled * own_normed, axis=-1, keepdims=True))
    ).astype(jnp.bfloat16)

    for k in range(1, nr):
        arrived(gz.at[layer(-k)], gz_s.at[k - 1], gz_r.at[k - 1])
    dgain_ref[...] = jnp.sum(gz[...], axis=0)
    for copy in sent:
        copy.wait_send()


def put(a, b, c, a_out, b_out, c_out, sem):
    copies = [
        pltpu.make_async_copy(src, dst, sem.at[i])
        for i, (src, dst) in enumerate(((a, a_out), (b, b_out), (c, c_out)))
    ]
    for copy in copies:
        copy.start()
    for copy in copies:
        copy.wait()


def fused(nr, nf, inputs, cotangent, norm_gain, gate_weight, up_weight, down_weight):
    own, width = inputs.shape
    share = gate_weight.shape[1]
    ng = 2 * nf
    group, cols = ng * own, width // nr
    bf16, f32 = jnp.bfloat16, jnp.float32
    vmem = pl.BlockSpec(memory_space=pltpu.VMEM)
    hbm = pl.BlockSpec(memory_space=pltpu.HBM)
    dma = pltpu.SemaphoreType.DMA
    pair = lambda *n: [dma(n), dma(n)]
    results = pl.pallas_call(
        functools.partial(kernel, nr, nf),
        out_shape=(
            jax.ShapeDtypeStruct((own, width), bf16),
            jax.ShapeDtypeStruct((1, width), f32),
            jax.ShapeDtypeStruct((share, cols), f32),
        ),
        in_specs=[hbm] * 6,
        out_specs=(vmem,) * 3,
        scratch_shapes=[
            pltpu.VMEM((own, width), bf16),
            pltpu.VMEM((own, width), bf16),
            pltpu.VMEM((1, width), f32),
            pltpu.VMEM((share, width), bf16),
            pltpu.VMEM((share, width), bf16),
            pltpu.VMEM((share, width), bf16),
            pltpu.VMEM((group, width), bf16),
            pltpu.VMEM((group, width), bf16),
            pltpu.VMEM((nr - 1, group, cols), bf16),
            pltpu.VMEM((group, share), bf16),
            pltpu.VMEM((nr - 1, group, share), bf16),
            pltpu.VMEM((group, width), f32),
            pltpu.VMEM((group, width), f32),
            pltpu.VMEM((nf, 2, own, width), bf16),
            pltpu.VMEM((nf, own, width), bf16),
            pltpu.VMEM((nf - 1, own, width), bf16),
            pltpu.VMEM((nf - 1, own, width), bf16),
            pltpu.VMEM((1, width), f32),
            pltpu.VMEM((nr, 1, width), f32),
            pltpu.VMEM((1, width), f32),
            pltpu.VMEM((ng, 1, width), f32),
            dma((6,)),
        ]
        + pair(nf - 1) + pair(nf) + pair(nf - 1) + pair(nf)
        + pair(nr - 1) + pair(nf - 1) + pair(nf)
        + pair(nr - 1) + pair(PIECES) + pair(PIECES, nf - 1) + pair(nr - 1) + pair(ng - 1),
        compiler_params=pltpu.CompilerParams(
            collective_id=0, has_side_effects=True, vmem_limit_bytes=52 * 1024 * 1024
        ),
    )(*[
        pltpu.with_memory_space_constraint(a, pltpu.HBM)
        for a in (
            inputs, cotangent, norm_gain[None], gate_weight.T, up_weight.T, down_weight
        )
    ])
    dx, dgain, ddown = pl.pallas_call(
        put,
        out_shape=tuple(jax.ShapeDtypeStruct(a.shape, a.dtype) for a in results),
        in_specs=[vmem] * 3,
        out_specs=(hbm,) * 3,
        scratch_shapes=[dma((3,))],
        compiler_params=pltpu.CompilerParams(vmem_limit_bytes=52 * 1024 * 1024),
    )(*results)
    return dx, dgain[0], ddown


def solution(mesh):
    nr, nf, nt = (mesh.shape[name] for name in ("rep", "fs", "tp"))

    def body(inputs, *others):
        block = inputs.shape[1] // nr
        if nt == 2 and nr > 1 and nf > 1 and block % LANES == 0 and inputs.shape[0] % 16 == 0:
            return fused(nr, nf, inputs, *others)
        return per_device(inputs, *others)

    return jax.shard_map(
        body,
        mesh=mesh,
        in_specs=(
            P(("rep", "fs", "tp"), None),
            P(("rep", "fs", "tp"), None),
            P(),
            P(None, ("fs", "tp")),
            P(None, ("fs", "tp")),
            P(("fs", "tp"), None),
        ),
        out_specs=(P(("rep", "fs", "tp"), None), P(), P(("fs", "tp"), "rep")),
        check_vma=False,
    )
```

profile of v0, /device:TPU:0, one launch (start us, length us, event | category | flops | bytes accessed | tf_op | source)
XLA Modules:
  0.0 26.5 jit_solution(9919985528432722905)
XLA Ops:
  0.6 25.0 %shard_map.85 = (bf16[16,2048]{1,0:T(8,128)(2,1)S(1)}, f32[1,2048]{1,0:T(1,128)S(1)}, f32[352,512]{1,0:T(8,128)S(1)}) custom-call(bf16[16,2048]{1,0:T(8,128)(2,1)} %x_hbm.1, bf16[16,2048]{1,0:T(8,128)(2,1)} %dy_hbm.1, f32[1,2048]{1,0:T(1,128)} %bitcast.6, bf16[352,2048]{1,0:T(8,128)(2,1)} %bitcast.4, bf16[352,2048]{1,0:T(8,128)(2,1)} %bitcast.5, ...), custom_call_target="tpu_custom_call" | custom-call | tf_op jit(solution)/shard_map/pallas_call | solution.py:288
  25.6 0.9 %shard_map.86 = (bf16[16,2048]{1,0:T(8,128)(2,1)}, f32[1,2048]{1,0:T(1,128)}, f32[352,512]{1,0:T(8,128)}) custom-call(bf16[16,2048]{1,0:T(8,128)(2,1)S(1)} %get-tuple-element.9.a, f32[1,2048]{1,0:T(1,128)S(1)} %get-tuple-element.10.b, f32[352,512]{1,0:T(8,128)S(1)} %get-tuple-element.11.c), custom_call_target="tpu_custom_call" | custom-call | tf_op jit(solution)/shard_map/pallas_call | solution.py:333
where the time goes:
time: 26.7 us; the launch traced here: 26.5 us
  Pallas kernels  25.9 us (97%)
  between operations  0.64 us (2%)
    pallas_call x1, Pallas kernels, fused(): pl.pallas_call(functools.partial(kernel, nr, nf), out_shape=(jax.ShapeDty...  25 us
    pallas_call x1, Pallas kernels, fused(): pl.pallas_call(put, out_shape=tuple((jax.ShapeDtypeStruct(a.shape, a.dtyp...  0.91 us

commit v1 on v0

v1 whole, which is shorter than its diff:
```python
import functools

import jax
import jax.numpy as jnp
from jax import lax
from jax.experimental import pallas as pl
from jax.experimental.pallas import tpu as pltpu
from jax.sharding import PartitionSpec as P

EPS = 1e-06


def across_tokens(left, right):
    return lax.dot_general(
        left, right, (((0,), (0,)), ((), ())), preferred_element_type=jnp.float32
    )


def across_columns(left, right):
    return lax.dot_general(
        left, right, (((1,), (1,)), ((), ())), preferred_element_type=jnp.float32
    )


def per_device(inputs, cotangent, norm_gain, gate_weight, up_weight, down_weight):
    whole_x, whole_dy = (
        lax.all_gather(inputs, ("fs", "tp"), axis=0, tiled=True),
        lax.all_gather(cotangent, ("fs", "tp"), axis=0, tiled=True),
    )
    xf = whole_x.astype(jnp.float32)
    inv = lax.rsqrt(jnp.mean(xf * xf, axis=-1, keepdims=True) + EPS)
    normed = xf * inv
    hidden_in = (normed * norm_gain).astype(jnp.bfloat16)
    gate = jnp.dot(hidden_in, gate_weight, preferred_element_type=jnp.float32)
    up = jnp.dot(hidden_in, up_weight, preferred_element_type=jnp.float32)
    sig = jax.nn.sigmoid(gate)
    act = gate * sig
    hidden = (act * up).astype(jnp.bfloat16)
    d_hidden = 0.5 * across_columns(whole_dy, down_weight)
    d_gate = (d_hidden * up * sig * (1.0 + gate * (1.0 - sig))).astype(jnp.bfloat16)
    d_up = (d_hidden * act).astype(jnp.bfloat16)
    own_rows = inputs.shape[0]
    d_in = lax.psum_scatter(
        across_columns(d_gate, gate_weight) + across_columns(d_up, up_weight),
        ("fs", "tp"),
        scatter_dimension=0,
        tiled=True,
    )
    offset = lax.axis_index(("fs", "tp")) * own_rows
    own_normed = lax.dynamic_slice_in_dim(normed, offset, own_rows, 0)
    own_inv = lax.dynamic_slice_in_dim(inv, offset, own_rows, 0)
    gain_grad = lax.psum(jnp.sum(d_in * own_normed, axis=0), ("rep", "fs", "tp"))
    scaled = d_in * norm_gain
    input_grad = (
        own_inv * (scaled - own_normed * jnp.mean(scaled * own_normed, axis=-1, keepdims=True))
    ).astype(jnp.bfloat16)
    input_grad, gain_grad = (input_grad, gain_grad)
    part_down = 0.5 * across_tokens(whole_dy, hidden)
    got_down = lax.all_to_all(
        part_down[None].astype(jnp.bfloat16), "rep", split_axis=1, concat_axis=0, tiled=True
    ).astype(jnp.float32)
    down_grad = jnp.sum(got_down, axis=0).T
    return (input_grad, gain_grad, down_grad)


MESH = pl.DeviceIdType.MESH
LANES = 128
PIECES = 4
LAYERS = 4
CHIPS = 4


def flip(i, k):
    return (i, i + 1 - 2 * lax.rem(i, 2), lax.rem(i + 2, 4), 3 - i)[k]


def tree(parts):
    while len(parts) > 1:
        parts = [parts[i] + parts[i + 1] for i in range(0, len(parts), 2)]
    return parts[0]


def kernel(
    x_hbm, dy_hbm, gain_hbm, wg_hbm, wu_hbm, wd_hbm,
    dx_ref, dgain_ref, ddown_ref,
    x_ref, dy_ref, gain_ref, w, wd, xg, dyg, dyc, own_hid, hid, normed, act_s, slope_s, dgu,
    d_in, d_out, d_pair, d_send, d_got, gz, gg,
    w_sem, out_sem, x_r, y_r, xs_r, ys_r, cz_r, c_r, cs_r, h_r, p_r, d_r, gg_r, gz_r, up_sem, down_sem,
):
    r, f, t = lax.axis_index("rep"), lax.axis_index("fs"), lax.axis_index("tp")
    own, width = x_hbm.shape
    share = wd.shape[0]
    cols = ddown_ref.shape[1]
    half = width // 2
    tokens = 2 * CHIPS * own
    sibling = (r, f, 1 - t)
    halves = (slice(0, half), slice(half, width))

    def chip(j):
        return (r, flip(f, j), t)

    def layer(k):
        return (flip(r, k), f, t)

    def span(p):
        return pl.ds(pl.multiple_of(p * cols, LANES), cols)

    def send(src, dst, ssem, rsem, to):
        pltpu.make_async_remote_copy(
            src_ref=src, dst_ref=dst, send_sem=ssem, recv_sem=rsem,
            device_id=to, device_id_type=MESH,
        ).start()

    def arrived(dst, rsem):
        pltpu.make_async_remote_copy(
            src_ref=dst, dst_ref=dst, send_sem=rsem, recv_sem=rsem,
            device_id=sibling, device_id_type=MESH,
        ).wait_recv()

    def left(src, ssem):
        pltpu.make_async_remote_copy(
            src_ref=src, dst_ref=src, send_sem=ssem, recv_sem=ssem,
            device_id=sibling, device_id_type=MESH,
        ).wait_send()

    loads = [
        pltpu.make_async_copy(src, dst, w_sem.at[i])
        for i, (src, dst) in enumerate(
            (
                (x_hbm, x_ref), (dy_hbm, dy_ref), (gain_hbm, gain_ref),
                (wg_hbm, w.at[:share]), (wu_hbm, w.at[share:]), (wd_hbm, wd),
            )
        )
    ]
    for load in loads:
        load.start()

    def signal(sem, to):
        pl.semaphore_signal(sem, inc=1, device_id=to, device_id_type=MESH)

    barrier = pltpu.get_barrier_semaphore()
    below, above = r > 0, r < LAYERS - 1
    for to in (chip(1), chip(2), sibling):
        signal(barrier, to)

    @pl.when(below)
    def _():
        signal(barrier, (r - 1, f, t))

    @pl.when(above)
    def _():
        signal(barrier, (r + 1, f, t))

    pl.semaphore_wait(barrier, 3 + below.astype(jnp.int32) + above.astype(jnp.int32))

    bulk, part_out, hid_out, gg_out, gz_out = (out_sem.at[i] for i in range(5))

    loads[0].wait()
    loads[1].wait()
    pairs = ((x_ref, xg, x_r), (dy_ref, dyg, y_r))
    for turn in range(2):
        for ref, into, rs in pairs:
            for j in (1, 2):
                c = halves[(j + 1 + turn) % 2]
                send(ref.at[:, c], into.at[0, j, :, c], bulk, rs.at[2 * (j - 1) + turn], chip(j))
    send(x_ref, xg.at[1, 0], bulk, xs_r.at[0], sibling)
    send(dy_ref, dyg.at[1, 0], bulk, ys_r.at[0], sibling)

    for step in range(LAYERS - 2):
        @pl.when(jnp.logical_and(r > step, above))
        def _(step=step):
            signal(up_sem.at[step], (r + 1, f, t))

        @pl.when(jnp.logical_and(r < LAYERS - 1 - step, below))
        def _(step=step):
            signal(down_sem.at[step], (r - 1, f, t))

        @pl.when(r > step + 1)
        def _(step=step):
            pl.semaphore_wait(up_sem.at[step], 1)

        @pl.when(r < LAYERS - 2 - step)
        def _(step=step):
            pl.semaphore_wait(down_sem.at[step], 1)

    for k in range(1, LAYERS):
        send(dy_ref.at[:, span(flip(r, k))], dyc.at[k - 1, 0, 0], part_out, cz_r.at[0], layer(k))

    xg[0, 0] = x_ref[...]
    dyg[0, 0] = dy_ref[...]

    def forward(lo, hi):
        n = hi - lo
        xf = xg[:, lo:hi].reshape(2 * n * own, width).astype(jnp.float32)
        inv = lax.rsqrt(jnp.mean(xf * xf, axis=-1, keepdims=True) + EPS)
        xf = xf * inv
        normed[:, lo:hi] = xf.reshape(2, n, own, width)
        hidden_in = (xf * gain_ref[...]).astype(jnp.bfloat16)
        gate = across_columns(hidden_in, w[:share])
        up = across_columns(hidden_in, w[share:])
        sig = jax.nn.sigmoid(gate)
        act = gate * sig
        own_hid[:, lo:hi] = (act * up).astype(jnp.bfloat16).reshape(2, n, own, share)
        for k in range(1, LAYERS):
            send(own_hid.at[:, lo:hi], hid.at[k - 1, :, lo:hi], hid_out, h_r.at[k - 1], layer(k))
        act_s[:, lo:hi] = act.reshape(2, n, own, share)
        slope_s[:, lo:hi] = (up * sig * (1.0 + gate * (1.0 - sig))).reshape(2, n, own, share)

    def share_on(into, j, turn, rs, bs, relay):
        c = halves[(j + 1 + turn) % 2]
        block = into.at[0, j, :, c]
        arrived(block, rs)
        if relay is not None:
            send(block, into.at[0, 3, :, c], bulk, relay, chip(3 - j))
        send(block, into.at[1, j, :, c], bulk, bs, sibling)

    arrived(xg.at[1, 0], xs_r.at[0])
    for load in loads[2:5]:
        load.wait()
    forward(0, 1)

    for _, into, rs in pairs:
        bs = xs_r.at[1] if into is xg else ys_r.at[0]
        for j in (1, 2):
            share_on(into, j, 0, rs.at[2 * (j - 1)], bs, rs.at[3 + j])
    for _, into, rs in pairs:
        bs = xs_r.at[1] if into is xg else ys_r.at[0]
        for j in (1, 2):
            share_on(into, j, 1, rs.at[2 * (j - 1) + 1], bs, None)

    def diagonal(into, rs, bs):
        for j in (1, 2):
            c = halves[(j + 1) % 2]
            block = into.at[0, 3, :, c]
            arrived(block, rs.at[3 + j])
            send(block, into.at[1, 3, :, c], bulk, bs, sibling)

    diagonal(xg, x_r, xs_r.at[2])
    arrived(xg.at[1, 1:3], xs_r.at[1])
    forward(1, 3)
    diagonal(dyg, y_r, ys_r.at[0])

    arrived(dyc.at[:, 0, 0], cz_r.at[0])
    for j in (3, 1, 2):
        send(dyc.at[:, 0, 0], dyc.at[:, 0, j], part_out, c_r.at[0], chip(j))
    send(dyc.at[:, 0, 0], dyc.at[:, 1, 0], part_out, cs_r.at[0], sibling)

    arrived(xg.at[1, 3], xs_r.at[2])
    forward(3, 4)

    arrived(dyg.at[1], ys_r.at[0])
    loads[5].wait()
    d_hidden = 0.5 * across_columns(dyg[...].reshape(tokens, width), wd[...])
    dgu[:, :share] = (d_hidden * slope_s[...].reshape(tokens, share)).astype(jnp.bfloat16)
    dgu[:, share:] = (d_hidden * act_s[...].reshape(tokens, share)).astype(jnp.bfloat16)

    step = width // PIECES
    parts = [slice(p * step, (p + 1) * step) for p in range(PIECES)]
    for p, part in enumerate(parts):
        piece = jnp.dot(dgu[...], w[:, part], preferred_element_type=jnp.float32)
        shaped = piece.reshape(2, CHIPS, own, step)
        d_out[:, :, part] = shaped[1].astype(jnp.bfloat16)
        send(d_out.at[:, :, part], d_pair.at[:, :, part], bulk, p_r.at[p], sibling)
        d_in[:, :, part] = shaped[0]
        gg[0, :, part] = jnp.sum(
            piece * normed[:, :, :, part].reshape(tokens, step), axis=0, keepdims=True
        )
    for u in range(2):
        for j in range(CHIPS):
            if u or j:
                to = (r, flip(f, j), t + u * (1 - 2 * t))
                send(gg.at[0], gg.at[CHIPS * u + j], gg_out, gg_r.at[0], to)

    for p, part in enumerate(parts):
        arrived(d_pair.at[:, :, part], p_r.at[p])
        for j in (3, 1, 2):
            d_send[j - 1, :, part] = (
                d_in[j, :, part] + d_pair[j, :, part].astype(jnp.float32)
            ).astype(jnp.bfloat16)
            send(d_send.at[j - 1, :, part], d_got.at[j - 1, :, part], bulk, d_r.at[0], chip(j))

    arrived(dyc.at[:, 0, 1:], c_r.at[0])
    send(dyc.at[:, 0, 1:], dyc.at[:, 1, 1:], part_out, cs_r.at[0], sibling)

    arrived(gg.at[1:], gg_r.at[0])
    gz[0] = tree([gg[i] for i in range(2 * CHIPS)])
    for k in range(1, LAYERS):
        send(gz.at[0], gz.at[k], gz_out, gz_r.at[0], layer(k))

    total = across_tokens(
        own_hid[...].reshape(tokens, share), dyg[:, :, :, span(r)].reshape(tokens, cols)
    )
    mine = d_in[0] + d_pair[0].astype(jnp.float32)
    xf = x_ref[...].astype(jnp.float32)
    own_inv = lax.rsqrt(jnp.mean(xf * xf, axis=-1, keepdims=True) + EPS)
    own_normed = xf * own_inv

    arrived(dyc.at[:, 1], cs_r.at[0])
    for k in range(1, LAYERS):
        arrived(hid.at[k - 1], h_r.at[k - 1])
    rest = (LAYERS - 1) * tokens
    ddown_ref[...] = 0.5 * (
        total + across_tokens(hid[...].reshape(rest, share), dyc[...].reshape(rest, cols))
    )

    arrived(d_got, d_r.at[0])
    for j in range(1, CHIPS):
        mine = mine + d_got[j - 1].astype(jnp.float32)
    scaled = mine * gain_ref[...]
    dx_ref[...] = (
        own_inv * (scaled - own_normed * jnp.mean(scaled * own_normed, axis=-1, keepdims=True))
    ).astype(jnp.bfloat16)

    arrived(gz.at[1:], gz_r.at[0])
    dgain_ref[...] = tree([gz[k] for k in range(LAYERS)])

    blocks = 2 * (3 + 4) + 4 + 3
    left(w.at[: blocks * own], bulk)
    left(dyc, part_out)
    left(hid, hid_out)
    left(gg.at[1:], gg_out)
    left(gz.at[1:], gz_out)


def put(a, b, c, a_out, b_out, c_out, sem):
    copies = [
        pltpu.make_async_copy(src, dst, sem.at[i])
        for i, (src, dst) in enumerate(((a, a_out), (b, b_out), (c, c_out)))
    ]
    for copy in copies:
        copy.start()
    for copy in copies:
        copy.wait()


def fused(inputs, cotangent, norm_gain, gate_weight, up_weight, down_weight):
    own, width = inputs.shape
    share = gate_weight.shape[1]
    cols = width // LAYERS
    tokens = 2 * CHIPS * own
    bf16, f32 = jnp.bfloat16, jnp.float32
    vmem = pl.BlockSpec(memory_space=pltpu.VMEM)
    hbm = pl.BlockSpec(memory_space=pltpu.HBM)
    dma = pltpu.SemaphoreType.DMA
    results = pl.pallas_call(
        kernel,
        out_shape=(
            jax.ShapeDtypeStruct((own, width), bf16),
            jax.ShapeDtypeStruct((1, width), f32),
            jax.ShapeDtypeStruct((share, cols), f32),
        ),
        in_specs=[hbm] * 6,
        out_specs=(vmem,) * 3,
        scratch_shapes=[
            pltpu.VMEM((own, width), bf16),
            pltpu.VMEM((own, width), bf16),
            pltpu.VMEM((1, width), f32),
            pltpu.VMEM((2 * share, width), bf16),
            pltpu.VMEM((share, width), bf16),
            pltpu.VMEM((2, CHIPS, own, width), bf16),
            pltpu.VMEM((2, CHIPS, own, width), bf16),
            pltpu.VMEM((LAYERS - 1, 2, CHIPS, own, cols), bf16),
            pltpu.VMEM((2, CHIPS, own, share), bf16),
            pltpu.VMEM((LAYERS - 1, 2, CHIPS, own, share), bf16),
            pltpu.VMEM((2, CHIPS, own, width), f32),
            pltpu.VMEM((2, CHIPS, own, share), f32),
            pltpu.VMEM((2, CHIPS, own, share), f32),
            pltpu.VMEM((tokens, 2 * share), bf16),
            pltpu.VMEM((CHIPS, own, width), f32),
            pltpu.VMEM((CHIPS, own, width), bf16),
            pltpu.VMEM((CHIPS, own, width), bf16),
            pltpu.VMEM((CHIPS - 1, own, width), bf16),
            pltpu.VMEM((CHIPS - 1, own, width), bf16),
            pltpu.VMEM((LAYERS, 1, width), f32),
            pltpu.VMEM((2 * CHIPS, 1, width), f32),
            dma((6,)), dma((5,)),
            dma((6,)), dma((6,)), dma((3,)), dma((1,)),
            dma((1,)), dma((1,)), dma((1,)),
            dma((LAYERS - 1,)), dma((PIECES,)), dma((1,)), dma((1,)), dma((1,)),
            pltpu.SemaphoreType.REGULAR((LAYERS - 2,)),
            pltpu.SemaphoreType.REGULAR((LAYERS - 2,)),
        ],
        compiler_params=pltpu.CompilerParams(
            collective_id=0, has_side_effects=True, vmem_limit_bytes=52 * 1024 * 1024
        ),
    )(*[
        pltpu.with_memory_space_constraint(a, pltpu.HBM)
        for a in (
            inputs, cotangent, norm_gain[None], gate_weight.T, up_weight.T, down_weight
        )
    ])
    dx, dgain, ddown = pl.pallas_call(
        put,
        out_shape=tuple(jax.ShapeDtypeStruct(a.shape, a.dtype) for a in results),
        in_specs=[vmem] * 3,
        out_specs=(hbm,) * 3,
        scratch_shapes=[dma((3,))],
        compiler_params=pltpu.CompilerParams(vmem_limit_bytes=52 * 1024 * 1024),
    )(*results)
    return dx, dgain[0], ddown


def solution(mesh):
    nr, nf, nt = (mesh.shape[name] for name in ("rep", "fs", "tp"))

    def body(inputs, *others):
        block = inputs.shape[1] // nr
        fits = nt == 2 and nr == LAYERS and nf == CHIPS
        if fits and block % LANES == 0 and inputs.shape[0] % 16 == 0:
            return fused(inputs, *others)
        return per_device(inputs, *others)

    return jax.shard_map(
        body,
        mesh=mesh,
        in_specs=(
            P(("rep", "fs", "tp"), None),
            P(("rep", "fs", "tp"), None),
            P(),
            P(None, ("fs", "tp")),
            P(None, ("fs", "tp")),
            P(("fs", "tp"), None),
        ),
        out_specs=(P(("rep", "fs", "tp"), None), P(), P(("fs", "tp"), "rep")),
        check_vma=False,
    )
```

time: 26.7 us -> 24.3 us (0.910)
  Pallas kernels: 25.9 us -> 23.5 us
    pallas_call x1, Pallas kernels: 25 us -> 22.6 us  [fused(): pl.pallas_call(kernel, out_shape=(jax.ShapeDtypeStruct((own, width), bf16...]
where the time goes in v1:
time: 24.3 us; the launch traced here: 24.1 us
  Pallas kernels  23.5 us (97%)
  between operations  0.64 us (3%)
    pallas_call x1, Pallas kernels, fused(): pl.pallas_call(kernel, out_shape=(jax.ShapeDtypeStruct((own, width), bf16...  22.6 us
    pallas_call x1, Pallas kernels, fused(): pl.pallas_call(put, out_shape=tuple((jax.ShapeDtypeStruct(a.shape, a.dtyp...  0.91 us

profile of v1, /device:TPU:0, one launch (start us, length us, event | category | flops | bytes accessed | tf_op | source)
XLA Modules:
  0.0 24.1 jit_solution(6868498523021909854)
XLA Ops:
  0.6 22.6 %shard_map.85 = (bf16[16,2048]{1,0:T(8,128)(2,1)S(1)}, f32[1,2048]{1,0:T(1,128)S(1)}, f32[352,512]{1,0:T(8,128)S(1)}) custom-call(bf16[16,2048]{1,0:T(8,128)(2,1)} %x_hbm.1, bf16[16,2048]{1,0:T(8,128)(2,1)} %dy_hbm.1, f32[1,2048]{1,0:T(1,128)} %bitcast.6, bf16[352,2048]{1,0:T(8,128)(2,1)} %bitcast.4, bf16[352,2048]{1,0:T(8,128)(2,1)} %bitcast.5, ...), custom_call_target="tpu_custom_call" | custom-call | tf_op jit(solution)/shard_map/pallas_call | solution.py:345
  23.2 0.9 %shard_map.86 = (bf16[16,2048]{1,0:T(8,128)(2,1)}, f32[1,2048]{1,0:T(1,128)}, f32[352,512]{1,0:T(8,128)}) custom-call(bf16[16,2048]{1,0:T(8,128)(2,1)S(1)} %get-tuple-element.9.a, f32[1,2048]{1,0:T(1,128)S(1)} %get-tuple-element.10.b, f32[352,512]{1,0:T(8,128)S(1)} %get-tuple-element.11.c), custom_call_target="tpu_custom_call" | custom-call | tf_op jit(solution)/shard_map/pallas_call | solution.py:392
